TPU v7x, 32 devices: a whole 2x2x4 slice. The times are simulated.
32 devices in a mesh: kv: 8 (over z, x), tp: 4 (over y, core).
Axes of the slice: x: 2, y: 2, z: 4, core: 2. Of those that a mesh axis runs over, the one named last changes fastest.
Arguments:
- tokens: bfloat16 [256, 4096], P(None, ('kv', 'tp')), may hold values from -6 to 6
- previous_state: float32 [256, 32, 128, 128], P('kv', 'tp'), may hold values from -6 to 6
- lengths: int32 [256], P('kv'), may hold values from 1 to 16384, 1048576 in all
- first_feed_norm_gain: float32 [4096], replicated, may hold values from 0.1 to 1.9
- first_gate_projection: bfloat16 [4096, 11264], P('kv', 'tp'), may hold values from -0.09375 to 0.09375
- first_up_projection: bfloat16 [4096, 11264], P('kv', 'tp'), may hold values from -0.09375 to 0.09375
- first_down_projection: bfloat16 [11264, 4096], P('tp', 'kv'), may hold values from -0.078125 to 0.078125
- mixer_norm_gain: float32 [4096], replicated, may hold values from 0.1 to 1.9
- query_weight: bfloat16 [4096, 4096], P('kv', 'tp'), may hold values from -0.09375 to 0.09375
- key_weight: bfloat16 [4096, 4096], P('kv', 'tp'), may hold values from -0.09375 to 0.09375
- value_weight: bfloat16 [4096, 4096], P('kv', 'tp'), may hold values from -0.09375 to 0.09375
- output_gate_weight: bfloat16 [4096, 4096], P('kv', 'tp'), may hold values from -0.09375 to 0.09375
- write_strength_weight: bfloat16 [4096, 32], replicated, may hold values from -0.09375 to 0.09375
- decay_input_weight: bfloat16 [4096, 32], replicated, may hold values from -0.09375 to 0.09375
- head_log_decay_rate: float32 [32], P('tp'), may hold values from -5 to 1
- decay_input_bias: float32 [32], P('tp'), may hold values from -1 to 1
- length_span_bias: float32 [32, 17], P('tp'), may hold values from -2 to 2
- extra_log_decay: float32 [256, 32], P('kv', 'tp'), may hold values from -0.7 to 0
- readout_head_norm_gain: float32 [128], replicated, may hold values from 0.1 to 1.9
- mixer_output_weight: bfloat16 [4096, 4096], P('tp', 'kv'), may hold values from -0.125 to 0.125
- second_feed_norm_gain: float32 [4096], replicated, may hold values from 0.1 to 1.9
- second_gate_projection: bfloat16 [4096, 11264], P('kv', 'tp'), may hold values from -0.09375 to 0.09375
- second_up_projection: bfloat16 [4096, 11264], P('kv', 'tp'), may hold values from -0.09375 to 0.09375
- second_down_projection: bfloat16 [11264, 4096], P('tp', 'kv'), may hold values from -0.078125 to 0.078125
Outputs:
- result: bfloat16 [256, 4096], P(None, ('kv', 'tp'))
- new_state: float32 [256, 32, 128, 128], P('kv', 'tp')
All inputs are finite; a program needn't handle non-finite values. No bound on the sum of `lengths` on one device may be relied on, other than what follows from the above.
Results may differ from a plain program's by a relative error of at most 0.03.
Values may be sent and summed in bfloat16 or wider, within the bound.
A program may use at most 128 MiB of HBM per device.

v0:
```python
import functools

import jax
import jax.numpy as jnp
from jax import lax
from jax.experimental import pallas as pl
from jax.experimental.pallas import tpu as pltpu
from jax.sharding import PartitionSpec as P

SPAN = 1024


EPSILON = 1e-06


LANES = 128


def part_of(ref, index, size, dim):
    window = pl.ds(pl.multiple_of(index * size, size), size)
    return ref.at[window] if dim == 0 else ref.at[:, window]


def meet(axis, me, n):
    barrier = pltpu.get_barrier_semaphore()
    for away in range(1, n):
        pl.semaphore_signal(
            barrier,
            inc=1,
            device_id={axis: lax.rem(me + away, n)},
            device_id_type=pl.DeviceIdType.MESH,
        )
    pl.semaphore_wait(barrier, n - 1)


def reduce_kernel(axis, n, dim, count, *refs):
    sources, sums = refs[:count], refs[count : 2 * count]
    slots = refs[2 * count : 3 * count]
    send_sem, recv_sem = refs[3 * count :]
    me = lax.axis_index(axis)
    meet(axis, me, n)
    copies = []
    for item, (source, slot) in enumerate(zip(sources, slots)):
        size = slot.shape[1 + dim]
        for away in range(1, n):
            peer = lax.rem(me + away, n)
            copy = pltpu.make_async_remote_copy(
                src_ref=part_of(source, peer, size, dim),
                dst_ref=slot.at[away - 1],
                send_sem=send_sem.at[item, away - 1],
                recv_sem=recv_sem.at[item, away - 1],
                device_id={axis: peer},
                device_id_type=pl.DeviceIdType.MESH,
            )
            copy.start()
            copies.append(copy)
    for item, (source, slot, total) in enumerate(zip(sources, slots, sums)):
        for copy in copies[item * (n - 1) : (item + 1) * (n - 1)]:
            copy.wait()
        own = part_of(source, me, slot.shape[1 + dim], dim)

        def add(step, carry, own=own, slot=slot, total=total):
            columns = pl.ds(pl.multiple_of(step * LANES, LANES), LANES)
            value = own[:, columns].astype(jnp.float32)
            for away in range(n - 1):
                value = value + slot[away, :, columns].astype(jnp.float32)
            total[:, columns] = value
            return carry

        lax.fori_loop(0, total.shape[1] // LANES, add, 0)


def scatter_sums(arrays, axis, dim, call_id):
    n = lax.axis_size(axis)
    count = len(arrays)
    shapes = []
    for array in arrays:
        shape = list(array.shape)
        shape[dim] //= n
        shapes.append(tuple(shape))
    vmem = pl.BlockSpec(memory_space=pltpu.VMEM)
    return pl.pallas_call(
        functools.partial(reduce_kernel, axis, n, dim, count),
        out_shape=[jax.ShapeDtypeStruct(shape, jnp.float32) for shape in shapes],
        in_specs=[vmem] * count,
        out_specs=[vmem] * count,
        scratch_shapes=[
            pltpu.VMEM((n - 1,) + shape, array.dtype) for shape, array in zip(shapes, arrays)
        ]
        + [pltpu.SemaphoreType.DMA((count, n - 1))] * 2,
        compiler_params=pltpu.CompilerParams(collective_id=call_id, has_side_effects=True),
    )(*arrays)


def gather_kernel(axis, n, source, gathered, send_sem, recv_sem):
    me = lax.axis_index(axis)
    size = source.shape[0]
    meet(axis, me, n)
    copies = []
    for away in range(1, n):
        copy = pltpu.make_async_remote_copy(
            src_ref=source,
            dst_ref=part_of(gathered, me, size, 0),
            send_sem=send_sem.at[away - 1],
            recv_sem=recv_sem.at[away - 1],
            device_id={axis: lax.rem(me + away, n)},
            device_id_type=pl.DeviceIdType.MESH,
        )
        copy.start()
        copies.append(copy)
    gathered[pl.ds(pl.multiple_of(me * size, size), size)] = source[...]
    for copy in copies:
        copy.wait()


def gather_rows(array, axis, call_id):
    n = lax.axis_size(axis)
    vmem = pl.BlockSpec(memory_space=pltpu.VMEM)
    return pl.pallas_call(
        functools.partial(gather_kernel, axis, n),
        out_shape=jax.ShapeDtypeStruct((n * array.shape[0], array.shape[1]), array.dtype),
        in_specs=[vmem],
        out_specs=vmem,
        scratch_shapes=[pltpu.SemaphoreType.DMA((n - 1,))] * 2,
        compiler_params=pltpu.CompilerParams(collective_id=call_id, has_side_effects=True),
    )(array)


def total_over(products, axis, call_id):
    n = lax.axis_size(axis)
    parts = gather_rows(products.astype(jnp.bfloat16), axis, call_id)
    return jnp.sum(parts.reshape((n,) + products.shape).astype(jnp.float32), axis=0)


def ffn_block(block, gain_block, model_width, w_gate, w_up, w_down, call_id):
    values = block.astype(jnp.float32)
    squares = jnp.sum(values * values, axis=1, keepdims=True)
    scaled = (values * gain_block).astype(jnp.bfloat16)
    gate_part = jnp.dot(scaled, w_gate, preferred_element_type=jnp.float32)
    up_part = jnp.dot(scaled, w_up, preferred_element_type=jnp.float32)
    gate_share, up_share, totals = scatter_sums(
        [
            gate_part.astype(jnp.bfloat16),
            up_part.astype(jnp.bfloat16),
            jnp.broadcast_to(squares, (squares.shape[0], LANES)),
        ],
        "kv",
        0,
        call_id,
    )
    row_scale = lax.rsqrt(totals[:, :1] / model_width + EPSILON)
    hidden_share = (jax.nn.silu(row_scale * gate_share) * (row_scale * up_share)).astype(
        jnp.bfloat16
    )
    return jnp.dot(
        gather_rows(hidden_share, "kv", call_id + 1),
        w_down,
        preferred_element_type=jnp.float32,
    )


def unit_heads(raw):
    return raw * lax.rsqrt(jnp.sum(raw * raw, axis=-1, keepdims=True) + EPSILON)


def body(
    tokens,
    previous_state,
    lengths,
    first_feed_norm_gain,
    first_gate_projection,
    first_up_projection,
    first_down_projection,
    mixer_norm_gain,
    query_weight,
    key_weight,
    value_weight,
    output_gate_weight,
    write_strength_weight,
    decay_input_weight,
    head_log_decay_rate,
    decay_input_bias,
    length_span_bias,
    extra_log_decay,
    readout_head_norm_gain,
    mixer_output_weight,
    second_feed_norm_gain,
    second_gate_projection,
    second_up_projection,
    second_down_projection,
):
    kv_index = lax.axis_index("kv")
    tp_index = lax.axis_index("tp")
    own_cols = tokens.shape[1]
    block_cols = own_cols * lax.axis_size("tp")
    seq_dev = previous_state.shape[0]
    heads_dev = previous_state.shape[1]
    head_size = previous_state.shape[2]
    model_width = mixer_norm_gain.shape[0]
    block_start = kv_index * block_cols
    token_block = lax.all_gather(tokens, "tp", axis=1, tiled=True)
    gain_one = lax.dynamic_slice_in_dim(first_feed_norm_gain, block_start, block_cols, 0)
    products = ffn_block(
        token_block,
        gain_one,
        model_width,
        first_gate_projection,
        first_up_projection,
        first_down_projection,
        0,
    )
    summed = total_over(products, "tp", 2)
    first_block = (token_block.astype(jnp.float32) + 0.5 * summed).astype(jnp.bfloat16)
    block_values = first_block.astype(jnp.float32)
    squares_part = jnp.sum(block_values * block_values, axis=1, keepdims=True)
    block_gain = lax.dynamic_slice_in_dim(mixer_norm_gain, block_start, block_cols, 0)
    scaled = (block_values * block_gain).astype(jnp.bfloat16)
    beta_rows = lax.dynamic_slice(
        write_strength_weight, (block_start, tp_index * heads_dev), (block_cols, heads_dev)
    )
    decay_rows = lax.dynamic_slice(
        decay_input_weight, (block_start, tp_index * heads_dev), (block_cols, heads_dev)
    )

    def apply_projection(weight):
        return jnp.dot(scaled, weight, preferred_element_type=jnp.float32)

    part_query = apply_projection(query_weight)
    part_key = apply_projection(key_weight)
    part_value = apply_projection(value_weight)
    part_gate = apply_projection(output_gate_weight)
    small = jnp.concatenate(
        [apply_projection(beta_rows), apply_projection(decay_rows), squares_part], axis=1
    )
    small = jnp.pad(small, ((0, 0), (0, -small.shape[1] % LANES)))
    query_raw, key_raw, value_raw, gate_raw, small_raw = scatter_sums(
        [
            part_query.astype(jnp.bfloat16),
            part_key.astype(jnp.bfloat16),
            part_value.astype(jnp.bfloat16),
            part_gate.astype(jnp.bfloat16),
            small,
        ],
        "kv",
        0,
        3,
    )
    beta_raw = small_raw[:, :heads_dev]
    decay_raw = small_raw[:, heads_dev : 2 * heads_dev]
    mine_total = small_raw[:, 2 * heads_dev : 2 * heads_dev + 1]
    row_scale = lax.rsqrt(mine_total / model_width + EPSILON)

    def split_heads(raw):
        return (row_scale * raw).reshape(seq_dev, heads_dev, head_size)

    queries = unit_heads(jax.nn.silu(split_heads(query_raw))) * head_size ** (-0.5)
    key_heads = unit_heads(jax.nn.silu(split_heads(key_raw)))
    value_heads = jax.nn.silu(split_heads(value_raw))
    out_gate = jax.nn.silu(split_heads(gate_raw))
    beta_gate = jax.nn.sigmoid(row_scale * beta_raw)
    span_index = lengths // SPAN
    matches = (
        span_index[:, None, None]
        == jnp.arange(length_span_bias.shape[1], dtype=jnp.int32)[None, None, :]
    )
    span_decay_bias = jnp.sum(jnp.where(matches, length_span_bias[None], 0.0), axis=2)
    decay_logarithm = (
        -jnp.exp(head_log_decay_rate)
        * jax.nn.softplus(row_scale * decay_raw + decay_input_bias + span_decay_bias)
        + extra_log_decay
    )
    held_state = jnp.exp(decay_logarithm)[..., None, None] * previous_state
    predicted = jnp.einsum("bhkv,bhk->bhv", held_state, key_heads, precision=lax.Precision.HIGHEST)
    new_state = (
        held_state
        + beta_gate[..., None, None]
        * key_heads[..., None]
        * (value_heads - predicted)[..., None, :]
    )
    readout = jnp.einsum("bhkv,bhk->bhv", new_state, queries, precision=lax.Precision.HIGHEST)
    readout = (
        readout
        * lax.rsqrt(jnp.mean(readout * readout, axis=-1, keepdims=True) + EPSILON)
        * readout_head_norm_gain
        * out_gate
    )
    mixed = readout.reshape(seq_dev, heads_dev * head_size).astype(jnp.bfloat16)
    mix_part = jnp.dot(
        gather_rows(mixed, "kv", 4),
        mixer_output_weight,
        preferred_element_type=jnp.float32,
    )
    mix_block = total_over(mix_part, "tp", 5)
    second_block = (block_values + mix_block).astype(jnp.bfloat16)
    gain_two = lax.dynamic_slice_in_dim(second_feed_norm_gain, block_start, block_cols, 0)
    products_two = ffn_block(
        second_block,
        gain_two,
        model_width,
        second_gate_projection,
        second_up_projection,
        second_down_projection,
        6,
    )
    if own_cols % LANES == 0:
        (summed_two,) = scatter_sums([products_two.astype(jnp.bfloat16)], "tp", 1, 8)
    else:
        summed_two = lax.dynamic_slice_in_dim(
            total_over(products_two, "tp", 8), tp_index * own_cols, own_cols, 1
        )
    second_own = lax.dynamic_slice_in_dim(second_block, tp_index * own_cols, own_cols, 1)
    result = (second_own.astype(jnp.float32) + 0.5 * summed_two).astype(jnp.bfloat16)
    return (result, new_state)


def solution(mesh):
    return jax.shard_map(
        body,
        mesh=mesh,
        in_specs=(
            P(None, ("kv", "tp")),
            P("kv", "tp", None, None),
            P("kv"),
            P(),
            P("kv", "tp"),
            P("kv", "tp"),
            P("tp", "kv"),
            P(),
            P("kv", "tp"),
            P("kv", "tp"),
            P("kv", "tp"),
            P("kv", "tp"),
            P(),
            P(),
            P("tp"),
            P("tp"),
            P("tp", None),
            P("kv", "tp"),
            P(),
            P("tp", "kv"),
            P(),
            P("kv", "tp"),
            P("kv", "tp"),
            P("tp", "kv"),
        ),
        out_specs=(P(None, ("kv", "tp")), P("kv", "tp", None, None)),
        check_vma=False,
    )
```

profile of v0, /device:TPU:1, one launch (start us, length us, event | category | flops | bytes accessed | tf_op | source)
XLA Modules:
  0.0 420.7 jit_solution(15567433318692460988)
XLA Ops:
  6.2 7.5 %all_gather.3 = bf16[256,512]{1,0:T(8,128)(2,1)S(1)} all-gather(bf16[256,128]{1,0:T(8,128)(2,1)} %param.24), channel_id=1, replica_groups=mesh['kv'=8,'tp'=4] {'tp'}, dimensions={1}, use_global_device_ids=true | all-gather | bytes 327680 | tf_op jit(solution)/shard_map/all_gather | solution.py:201
  14.5 2.0 convolution_convert_fusion.2.refs_1_
  16.6 2.0 convolution_convert_fusion.3.refs_0_
  18.6 72.5 %shard_map.239 = (f32[32,2816]{1,0:T(8,128)}, f32[32,2816]{1,0:T(8,128)}, f32[32,128]{1,0:T(8,128)}) custom-call(bf16[256,2816]{1,0:T(8,128)(2,1)} %convolution_convert_fusion.3.refs_0_, bf16[256,2816]{1,0:T(8,128)(2,1)} %convolution_convert_fusion.2.refs_1_, f32[256,128]{1,0:T(8,128)} %broadcast_in_dim.26.refs_2_), custom_call_target="tpu_custom_call" | custom-call | tf_op jit(solution)/shard_map/pallas_call | solution.py:82
  92.0 2.0 multiply_convert_fusion.1.source
  93.9 27.5 %shard_map.240 = bf16[256,2816]{1,0:T(8,128)(2,1)} custom-call(bf16[32,2816]{1,0:T(8,128)(2,1)} %multiply_convert_fusion.1.source), custom_call_target="tpu_custom_call" | custom-call | tf_op jit(solution)/shard_map/pallas_call | solution.py:119
  121.4 3.9 convolution_convert_fusion.10.source
  125.2 17.6 %shard_map.241 = bf16[1024,512]{1,0:T(8,128)(2,1)} custom-call(bf16[256,512]{1,0:T(8,128)(2,1)} %convolution_convert_fusion.10.source), custom_call_target="tpu_custom_call" | custom-call | tf_op jit(solution)/shard_map/pallas_call | solution.py:119
  142.9 1.5 convert_reduce_fusion.1
  147.2 1.3 convolution_convert_fusion.5.refs_2_
  148.4 1.3 convolution_convert_fusion.4.refs_3_
  149.7 2.5 convolution_convert_fusion.6.refs_1_
  152.1 1.2 convolution_convert_fusion.7.refs_0_
  153.4 62.9 %shard_map.242 = (f32[32,1024]{1,0:T(8,128)}, f32[32,1024]{1,0:T(8,128)}, f32[32,1024]{1,0:T(8,128)}, f32[32,1024]{1,0:T(8,128)}, f32[32,128]{1,0:T(8,128)}) custom-call(bf16[256,1024]{1,0:T(8,128)(2,1)} %convolution_convert_fusion.7.refs_0_, bf16[256,1024]{1,0:T(8,128)(2,1)} %convolution_convert_fusion.6.refs_1_, ...), custom_call_target="tpu_custom_call" | custom-call | tf_op jit(solution)/shard_map/pallas_call | solution.py:82
  216.3 0.9 rsqrt_reduce_fusion.1
  217.2 1.2 multiply_bitcast_fusion.1
  218.7 0.9 fusion.40
  219.8 18.4 %fusion = f32[32,8,1,128]{3,2,1,0:T(1,128)S(1)} fusion(f32[32,8,128,1]{2,3,1,0:T(1,128)S(1)} %bitcast.107, f32[32,8,128,128]{3,2,1,0:T(8,128)} %param.25, f32[32,8]{1,0:T(8,128)S(1)} %get-tuple-element.30), kind=kOutput, calls=%fused_computation.1 | convolution fusion | flops 54525952 | bytes 17040384 | tf_op jit(solution)/shard_map/bhkv,bhk->bhv/dot_general | solution.py:273
  238.7 6.0 %multiply_add_fusion = f32[32,8,128,128]{3,2,1,0:T(8,128)S(1)} fusion(f32[32,8,128,128]{3,2,1,0:T(8,128)S(1)} %bitcast.100, f32[32,8,128]{2,1,0:T(8,128)S(1)} %fusion.25, f32[32,8,128]{2,1,0:T(8,128)S(1)} %get-tuple-element.26, f32[32,8]{1,0:T(8,128)S(1)} %get-tuple-element.30), kind=kLoop, calls=%fused_computation | loop fusion | flops 12582912 | bytes 33817600 | tf_op jit(solution)/shard_map/add | solution.py:275
  244.7 14.7 %fusion.45 = f32[32,8,1,128]{3,2,1,0:T(1,128)S(1)} fusion(f32[32,8,128,128]{3,2,1,0:T(8,128)S(1)} %multiply_add_fusion, f32[32,8,128,1]{2,3,1,0:T(1,128)S(1)} %bitcast.106), kind=kOutput, calls=%fused_computation.93 | convolution fusion | flops 50331648 | bytes 17039360 | tf_op jit(solution)/shard_map/bhkv,bhk->bhv/dot_general | solution.py:280
  260.3 13.6 %shard_map.243 = bf16[256,1024]{1,0:T(8,128)(2,1)} custom-call(bf16[32,1024]{1,0:T(8,128)(2,1)} %bitcast.108), custom_call_target="tpu_custom_call" | custom-call | tf_op jit(solution)/shard_map/pallas_call | solution.py:119
  273.9 2.2 convolution_convert_fusion.9.source
  276.1 17.0 %shard_map.244 = bf16[1024,512]{1,0:T(8,128)(2,1)} custom-call(bf16[256,512]{1,0:T(8,128)(2,1)} %convolution_convert_fusion.9.source), custom_call_target="tpu_custom_call" | custom-call | tf_op jit(solution)/shard_map/pallas_call | solution.py:119
  293.1 1.4 convert_reduce_fusion
  295.4 3.8 convolution_convert_fusion.refs_1_
  299.3 2.1 convolution_convert_fusion.1.refs_0_
  301.3 74.1 %shard_map.245 = (f32[32,2816]{1,0:T(8,128)}, f32[32,2816]{1,0:T(8,128)}, f32[32,128]{1,0:T(8,128)}) custom-call(bf16[256,2816]{1,0:T(8,128)(2,1)} %convolution_convert_fusion.1.refs_0_, bf16[256,2816]{1,0:T(8,128)(2,1)} %convolution_convert_fusion.refs_1_, f32[256,128]{1,0:T(8,128)} %broadcast_in_dim.31.refs_2_), custom_call_target="tpu_custom_call" | custom-call | tf_op jit(solution)/shard_map/pallas_call | solution.py:82
  376.3 1.9 multiply_convert_fusion.source
  378.2 29.4 %shard_map.246 = bf16[256,2816]{1,0:T(8,128)(2,1)} custom-call(bf16[32,2816]{1,0:T(8,128)(2,1)} %multiply_convert_fusion.source), custom_call_target="tpu_custom_call" | custom-call | tf_op jit(solution)/shard_map/pallas_call | solution.py:119
  407.7 3.9 convolution_convert_fusion.8.refs_0_
  411.5 7.6 %shard_map.247 = f32[256,128]{1,0:T(8,128)} custom-call(bf16[256,512]{1,0:T(8,128)(2,1)} %convolution_convert_fusion.8.refs_0_), custom_call_target="tpu_custom_call" | custom-call | tf_op jit(solution)/shard_map/pallas_call | solution.py:82
  419.1 1.6 add_convert_fusion
  (69 shorter events, 13.3 us)
Async XLA Ops:
  0.6 13.9 %copy-start = (bf16[512,2816]{1,0:T(8,128)(2,1)S(1)}, bf16[512,2816]{1,0:T(8,128)(2,1)}, u32[]{:S(2)}) copy-start(bf16[512,2816]{1,0:T(8,128)(2,1)} %param.29) | copy-start | bytes 8650756
  6.2 10.4 %copy-start.3 = (bf16[512,2816]{1,0:T(8,128)(2,1)S(1)}, bf16[512,2816]{1,0:T(8,128)(2,1)}, u32[]{:S(2)}) copy-start(bf16[512,2816]{1,0:T(8,128)(2,1)} %param.28) | copy-start | bytes 8650756
  125.2 21.9 %copy-start.6 = (bf16[512,1024]{1,0:T(8,128)(2,1)S(1)}, bf16[512,1024]{1,0:T(8,128)(2,1)}, u32[]{:S(2)}) copy-start(bf16[512,1024]{1,0:T(8,128)(2,1)} %param.34) | copy-start | bytes 3145732
  142.9 5.5 %copy-start.7 = (bf16[512,1024]{1,0:T(8,128)(2,1)S(1)}, bf16[512,1024]{1,0:T(8,128)(2,1)}, u32[]{:S(2)}) copy-start(bf16[512,1024]{1,0:T(8,128)(2,1)} %param.35) | copy-start | bytes 3145732
  146.5 5.6 %copy-start.8 = (bf16[512,1024]{1,0:T(8,128)(2,1)S(1)}, bf16[512,1024]{1,0:T(8,128)(2,1)}, u32[]{:S(2)}) copy-start(bf16[512,1024]{1,0:T(8,128)(2,1)} %param.32) | copy-start | bytes 3145732
  152.1 66.5 %copy-start.9 = (f32[8]{0:T(128)S(1)}, f32[8]{0:T(128)}, u32[]{:S(2)}) copy-start(f32[8]{0:T(128)} %param.39) | copy-start | bytes 100
  219.7 18.9 %slice-start = ((s8[16777216]{0:T(1024)(128)(4,1)}), s8[4194304]{0:T(1024)(128)(4,1)S(1)}, s32[]{:S(2)}) async-start(s8[16777216]{0:T(1024)(128)(4,1)} %bitcast.99), calls=%async_computation | async-start | bytes 8388608
  219.7 18.9 %slice-start.1 = ((s8[16777216]{0:T(1024)(128)(4,1)}), s8[4194304]{0:T(1024)(128)(4,1)S(1)}, s32[]{:S(2)}) async-start(s8[16777216]{0:T(1024)(128)(4,1)} %bitcast.99), calls=%async_computation.1 | async-start | bytes 8388608
  219.7 18.9 %slice-start.2 = ((s8[16777216]{0:T(1024)(128)(4,1)}), s8[4194304]{0:T(1024)(128)(4,1)S(1)}, s32[]{:S(2)}) async-start(s8[16777216]{0:T(1024)(128)(4,1)} %bitcast.99), calls=%async_computation.2 | async-start | bytes 8388608
  219.8 18.9 %slice-start.3 = ((s8[16777216]{0:T(1024)(128)(4,1)}), s8[4194304]{0:T(1024)(128)(4,1)S(1)}, s32[]{:S(2)}) async-start(s8[16777216]{0:T(1024)(128)(4,1)} %bitcast.99), calls=%async_computation.3 | async-start | bytes 8388608
  244.6 14.8 %copy-start.2 = (f32[32,8,128,128]{3,2,1,0:T(8,128)}, f32[32,8,128,128]{3,2,1,0:T(8,128)S(1)}, u32[]{:S(2)}) copy-start(f32[32,8,128,128]{3,2,1,0:T(8,128)S(1)} %multiply_add_fusion) | copy-start | bytes 50331652
  244.7 14.9 %copy-start.10 = (f32[128]{0:T(128)S(1)}, f32[128]{0:T(128)}, u32[]{:S(2)}) copy-start(f32[128]{0:T(128)} %param.42) | copy-start | bytes 1540
  244.7 29.2 %copy-start.5 = (bf16[1024,512]{1,0:T(8,128)(2,1)S(1)}, bf16[1024,512]{1,0:T(8,128)(2,1)}, u32[]{:S(2)}) copy-start(bf16[1024,512]{1,0:T(8,128)(2,1)} %param.43) | copy-start | bytes 3145732
  294.5 4.8 %copy-start.4 = (bf16[512,2816]{1,0:T(8,128)(2,1)S(1)}, bf16[512,2816]{1,0:T(8,128)(2,1)}, u32[]{:S(2)}) copy-start(bf16[512,2816]{1,0:T(8,128)(2,1)} %param.45) | copy-start | bytes 8650756
  378.2 42.4 %copy-start.1 = (bf16[512,2816]{1,0:T(8,128)(2,1)S(1)}, bf16[512,2816]{1,0:T(8,128)(2,1)}, u32[]{:S(2)}) copy-start(bf16[512,2816]{1,0:T(8,128)(2,1)} %param.29) | copy-start | bytes 8650756
where the time goes:
time: 429 us; the launch traced here: 421 us
  Pallas kernels  322 us (75%)
  matrix products  61 us (14%)
  other arithmetic  21.9 us (5%)
  blocking collectives  7.45 us (2%)
  local copies, waits for them, and re-layouts  7 us (2%)
    pallas_call x4, Pallas kernels, scatter_sums(): pl.pallas_call(functools.partial(reduce_kernel, axis, n, dim, count), out...  217 us
    pallas_call x5, Pallas kernels, gather_rows(): pl.pallas_call(functools.partial(gather_kernel, axis, n), out_shape=jax.S...  105 us
    dot_general x1, matrix products, body(): jnp.einsum('bhkv,bhk->bhv', held_state, key_heads, precision=lax.Precisio...  18.4 us
    dot_general x1, matrix products, body(): jnp.einsum('bhkv,bhk->bhv', new_state, queries, precision=lax.Precision.H...  14.7 us

commit v1 on v0

v1 whole, which is shorter than its diff:
```python
import functools
from types import SimpleNamespace

import jax
import jax.numpy as jnp
from jax import lax
from jax.experimental import pallas as pl
from jax.experimental.pallas import tpu as pltpu
from jax.sharding import PartitionSpec as P

SPAN = 1024


EPSILON = 1e-06


LANES = 128


LIMIT = 46 << 20


KV = "kv"


TP = "tp"


MESH = pl.DeviceIdType.MESH


def log2(n):
    return n.bit_length() - 1


def bit(value, place):
    return lax.rem(value // (1 << place), 2)


def orders(n):
    bits = log2(n)
    plain = tuple(range(bits))
    swapped = (1, 0) + tuple(range(2, bits)) if bits > 1 else plain
    return plain, swapped


def place_of(block, order):
    bits = len(order)
    return sum(((block >> b) & 1) << (bits - 1 - k) for k, b in enumerate(order))


def meet(kv, tp, n_kv, n_tp):
    barrier = pltpu.get_barrier_semaphore()
    for away in range(1, n_kv):
        pl.semaphore_signal(
            barrier, inc=1, device_id={KV: lax.rem(kv + away, n_kv)}, device_id_type=MESH
        )
    for away in range(1, n_tp):
        pl.semaphore_signal(
            barrier, inc=1, device_id={TP: lax.rem(tp + away, n_tp)}, device_id_type=MESH
        )
    pl.semaphore_wait(barrier, n_kv + n_tp - 2)


def to_kv(src, dst, send, recv, peer):
    return pltpu.make_async_remote_copy(
        src_ref=src,
        dst_ref=dst,
        send_sem=send,
        recv_sem=recv,
        device_id={KV: peer},
        device_id_type=MESH,
    )


def to_tp(src, dst, send, recv, peer):
    return pltpu.make_async_remote_copy(
        src_ref=src,
        dst_ref=dst,
        send_sem=send,
        recv_sem=recv,
        device_id={TP: peer},
        device_id_type=MESH,
    )


def sum_rows_start(refs, kv, n):
    copies = []
    for away in range(1, n):
        peer = lax.rem(kv + away, n)
        copy = to_kv(
            refs.row_part.at[peer],
            refs.row_slot.at[away - 1],
            refs.row_sem.at[0, away - 1],
            refs.row_sem.at[1, away - 1],
            peer,
        )
        copy.start()
        copies.append(copy)
    return copies


def sum_rows_finish(refs, copies, kv, n):
    for copy in copies:
        copy.wait_recv()
    total = refs.row_part[kv]
    for away in range(n - 1):
        total = total + refs.row_slot[away]
    return total


class Exchange:
    def __init__(self, refs, kv, n, chunks, plain_chunks):
        self.refs, self.kv, self.n = refs, kv, n
        self.chunks, self.plain_chunks = chunks, plain_chunks
        self.bits = log2(n)
        self.orders = orders(n)

    def mine(self, j, k):
        first, second = self.orders[0][k], self.orders[1][k]
        if first == second:
            return bit(self.kv, first)
        return jnp.where(j < self.plain_chunks, bit(self.kv, first), bit(self.kv, second))

    def peer(self, j, k):
        first, second = self.orders[0][k], self.orders[1][k]
        up = self.kv + (1 - 2 * bit(self.kv, first)) * (1 << first)
        if first == second:
            return up
        other = self.kv + (1 - 2 * bit(self.kv, second)) * (1 << second)
        return jnp.where(j < self.plain_chunks, up, other)

    def place(self, depth):
        total = 0
        for k in range(depth):
            total = total + bit(self.kv, k) * (self.n >> (k + 1))
        return total

    def scatter(self, j, k):
        return to_kv(
            self.refs.part[k].at[j, 1 - self.mine(j, k)],
            self.refs.slot[k].at[j],
            self.refs.scatter_sem.at[0, k, j],
            self.refs.scatter_sem.at[1, k, j],
            self.peer(j, k),
        )

    def gather(self, j, a):
        last = self.bits - 1 - a
        window = self.refs.full.at[j, pl.ds(self.place(self.bits - a), 1 << a)]
        return to_kv(
            window,
            window,
            self.refs.gather_sem.at[0, a, j],
            self.refs.gather_sem.at[1, a, j],
            self.kv + (1 - 2 * bit(self.kv, last)) * (1 << last),
        )

    def produce(self, product):
        rows = self.refs.slot[-1].shape[1]
        part = self.refs.part[0]
        half = self.n // 2
        for order, low, high in (
            (self.orders[0], 0, 1),
            (self.orders[1], self.plain_chunks, self.chunks),
            (self.orders[0], 1, self.plain_chunks),
        ):

            def step(j, carry, order=order):
                value = product(j)
                for block in range(self.n):
                    place = place_of(block, order)
                    start = (place % half) * rows
                    part[j, place // half, start : start + rows] = value[
                        block * rows : (block + 1) * rows
                    ].astype(part.dtype)
                self.scatter(j, 0).start()
                return carry

            if high > low:
                lax.fori_loop(low, high, step, 0)

    def reduce(self, j, k, finish):
        self.scatter(j, k - 1).wait_recv()
        total = self.refs.part[k - 1][j, self.mine(j, k - 1)].astype(jnp.float32)
        total = total + self.refs.slot[k - 1][j].astype(jnp.float32)
        if k < self.bits:
            part = self.refs.part[k]
            rows = total.shape[0] // 2
            part[j, 0] = total[:rows].astype(part.dtype)
            part[j, 1] = total[rows:].astype(part.dtype)
            self.scatter(j, k).start()
        else:
            full = self.refs.full
            full[j, self.place(self.bits)] = finish(j, total)
            self.gather(j, 0).start()

    def relay(self, j, a):
        self.gather(j, a - 1).wait_recv()
        self.gather(j, a).start()

    def run(self, finish):
        bits = self.bits

        def step(t, carry):
            @pl.when(t < self.plain_chunks)
            def _():
                self.reduce(t, 1, finish)

            @pl.when(t < self.chunks - self.plain_chunks)
            def _():
                self.reduce(self.plain_chunks + t, 1, finish)

            for lag in range(1, 2 * bits - 1):
                j = t - lag

                @pl.when(jnp.logical_and(j >= 0, j < self.chunks))
                def _(lag=lag, j=j):
                    if lag < bits:
                        self.reduce(j, lag + 1, finish)
                    else:
                        self.relay(j, lag - bits + 1)

            return carry

        lax.fori_loop(0, self.chunks + 2 * bits - 2, step, 0)

    def consume(self, total, weight, weight_wait):
        full = self.refs.full
        rows, width = full.shape[2], full.shape[3]
        total[...] = jnp.zeros_like(total)
        order = self.orders[0]

        def step(j, carry):
            weight_wait(j)
            self.gather(j, self.bits - 1).wait_recv()
            product = jnp.dot(
                full[j].reshape(self.n * rows, width),
                weight[j],
                preferred_element_type=jnp.float32,
            )
            for block in range(self.n):
                place = place_of(block, order)
                total[block * rows : (block + 1) * rows] += product[
                    place * rows : (place + 1) * rows
                ]
            return carry

        lax.fori_loop(0, self.chunks, step, 0)

    def drain(self):
        def step(j, carry):
            for k in range(self.bits):
                self.scatter(j, k).wait_send()
                self.gather(j, k).wait_send()
            return carry

        lax.fori_loop(0, self.chunks, step, 0)


def total_over_tp(refs, total, base, out, scale, tp, n_tp):
    half = total.shape[0] // 2
    core = bit(tp, 0)
    other = tp + 1 - 2 * core
    part, slot, sems = refs.tp_part, refs.tp_slot, refs.tp_sem
    part[0, 0] = total[:half].astype(part.dtype)
    part[0, 1] = total[half:].astype(part.dtype)
    copies = [to_tp(part.at[0, 1 - core], slot.at[0], sems.at[0, 0], sems.at[1, 0], other)]
    copies[-1].start()
    copies[-1].wait_recv()
    value = part[0, core].astype(jnp.float32) + slot[0].astype(jnp.float32)
    for place in range(1, log2(n_tp)):
        part[place, 0] = value.astype(part.dtype)
        peer = tp + (1 - 2 * bit(tp, place)) * (1 << place)
        copies.append(
            to_tp(part.at[place, 0], slot.at[place], sems.at[0, place], sems.at[1, place], peer)
        )
        copies[-1].start()
        copies[-1].wait_recv()
        value = part[place, 0].astype(jnp.float32) + slot[place].astype(jnp.float32)
    out[core] = (base[core].astype(jnp.float32) + scale * value).astype(out.dtype)
    last = log2(n_tp)
    copies.append(to_tp(out.at[core], out.at[core], sems.at[0, last], sems.at[1, last], other))
    copies[-1].start()
    copies[-1].wait_recv()
    return copies


def exchange_scratch(n, chunks, rows, cols, width):
    bits = log2(n)
    shapes = SimpleNamespace()
    shapes.part = [
        pltpu.VMEM((chunks, 2, rows >> (k + 1), cols), jnp.bfloat16) for k in range(bits)
    ]
    shapes.slot = [
        pltpu.VMEM((chunks, rows >> (k + 1), cols), jnp.bfloat16) for k in range(bits)
    ]
    shapes.full = pltpu.VMEM((chunks, n, rows // n, width), jnp.bfloat16)
    shapes.scatter_sem = pltpu.SemaphoreType.DMA((2, bits, chunks))
    shapes.gather_sem = pltpu.SemaphoreType.DMA((2, bits, chunks))
    shapes.row_part = pltpu.VMEM((n, rows // n, LANES), jnp.float32)
    shapes.row_slot = pltpu.VMEM((n - 1, rows // n, LANES), jnp.float32)
    shapes.row_sem = pltpu.SemaphoreType.DMA((2, n - 1))
    return shapes


def tp_scratch(n_tp, rows, cols):
    bits = log2(n_tp)
    return dict(
        tp_part=pltpu.VMEM((bits, 2, rows // 2, cols), jnp.bfloat16),
        tp_slot=pltpu.VMEM((bits, rows // 2, cols), jnp.bfloat16),
        tp_sem=pltpu.SemaphoreType.DMA((2, bits + 1)),
    )


def chunks_of(columns):
    tiles = columns // LANES
    return max(d for d in range(1, 13) if tiles % d == 0)


def plain_share(n, chunks):
    return chunks if log2(n) < 2 else chunks - (chunks + 2) // 6


def scale_rows(x, gain, scaled, kv):
    half, cols = x.shape[1:]
    columns = gain[:, pl.ds(pl.multiple_of(kv * cols, LANES), cols)]
    squares = []
    for side in range(2):
        values = x[side].astype(jnp.float32)
        squares.append(jnp.sum(values * values, axis=1, keepdims=True))
        scaled[side * half : (side + 1) * half] = (values * columns).astype(jnp.bfloat16)
    return jnp.concatenate(squares, axis=0)


class Feed:
    def __init__(self, refs, sources, kv, tp):
        self.refs, self.sources, self.kv, self.tp = refs, sources, kv, tp
        self.n, self.n_tp = lax.axis_size(KV), lax.axis_size(TP)
        self.chunks, self.width = refs.down.shape[:2]

    def fetch(self, j, side):
        columns = pl.ds(pl.multiple_of(j * self.width, LANES), self.width)
        return pltpu.make_async_copy(
            self.sources[side].at[:, columns],
            self.refs.weights.at[j, :, pl.ds(side * self.width, self.width)],
            self.refs.weight_sem.at[side, j],
        )

    def fetch_down(self, j):
        return pltpu.make_async_copy(
            self.sources[2].at[pl.ds(pl.multiple_of(j * self.width, LANES), self.width)],
            self.refs.down.at[j],
            self.refs.weight_sem.at[2, j],
        )

    def start_weights(self):
        def step(j, carry):
            self.fetch(j, 0).start()
            self.fetch(j, 1).start()
            return carry

        lax.fori_loop(0, self.chunks, step, 0)

    def start_down(self):
        def step(j, carry):
            self.fetch_down(j).start()
            return carry

        lax.fori_loop(0, self.chunks, step, 0)

    def run(self, x, gain, model_width):
        refs, kv, n, width = self.refs, self.kv, self.n, self.width
        squares = scale_rows(x, gain, refs.scaled, kv)
        rows = squares.shape[0]
        refs.row_part[...] = jnp.broadcast_to(squares, (rows, LANES)).reshape(
            n, rows // n, LANES
        )
        row_copies = sum_rows_start(refs, kv, n)
        exchange = Exchange(refs, kv, n, self.chunks, plain_share(n, self.chunks))

        def product(j):
            self.fetch(j, 0).wait()
            self.fetch(j, 1).wait()
            return jnp.dot(
                refs.scaled[...], refs.weights[j], preferred_element_type=jnp.float32
            )

        exchange.produce(product)
        totals = sum_rows_finish(refs, row_copies, kv, n)
        refs.row_scale[...] = lax.rsqrt(totals / model_width + EPSILON)

        def finish(j, sums):
            row_scale = refs.row_scale[:, :1]
            gate = row_scale * sums[:, :width]
            up = row_scale * sums[:, width:]
            return (jax.nn.silu(gate) * up).astype(jnp.bfloat16)

        exchange.run(finish)
        exchange.consume(refs.total, refs.down, lambda j: self.fetch_down(j).wait())

        def drain():
            exchange.drain()
            for copy in row_copies:
                copy.wait_send()

        return drain


def own_columns(refs, total, base, out, tp, n_tp):
    part, slot, sems = refs.out_part, refs.out_slot, refs.out_sem
    rows, own = part.shape[1:]
    half = rows // 2
    for piece in range(n_tp):
        part[piece] = total[:, piece * own : (piece + 1) * own].astype(part.dtype)
    copies = []
    for away in range(1, n_tp):
        peer = lax.rem(tp + away, n_tp)
        copy = to_tp(
            part.at[peer], slot.at[away - 1], sems.at[0, away - 1], sems.at[1, away - 1], peer
        )
        copy.start()
        copies.append(copy)
    value = part[tp].astype(jnp.float32)
    for away in range(1, n_tp):
        copies[away - 1].wait_recv()
        value = value + slot[away - 1].astype(jnp.float32)
    columns = pl.ds(pl.multiple_of(tp * own, LANES), own)
    for side in range(2):
        mine = base[side, :, columns].astype(jnp.float32)
        window = slice(side * half, (side + 1) * half)
        out[window] = (mine + 0.5 * value[window]).astype(out.dtype)
    return copies


class Mixer:
    def __init__(self, refs, io, kv, tp):
        self.refs, self.io, self.kv, self.tp = refs, io, kv, tp
        self.n, self.n_tp = lax.axis_size(KV), lax.axis_size(TP)
        self.heads, self.head_size, self.block_cols = refs.mix_out.shape
        self.slots = refs.state.shape[0]
        self.projections = (io.w_query, io.w_key, io.w_value, io.w_gate)

    def fetch(self, j, side):
        size = self.head_size
        return pltpu.make_async_copy(
            self.projections[side].at[:, pl.ds(pl.multiple_of(j * size, LANES), size)],
            self.refs.weights.at[j, :, pl.ds(side * size, size)],
            self.refs.weight_sem.at[side, j],
        )

    def fetch_mix(self, j):
        size = self.head_size
        return pltpu.make_async_copy(
            self.io.w_mix.at[pl.ds(pl.multiple_of(j * size, LANES), size)],
            self.refs.mix_out.at[j],
            self.refs.weight_sem.at[4, j],
        )

    def fetch_state(self, j):
        return pltpu.make_async_copy(
            self.io.previous.at[:, j],
            self.refs.state.at[lax.rem(j, self.slots)],
            self.refs.state_sem.at[j],
        )

    def fetch_small(self, side):
        start = pl.multiple_of(self.kv * self.block_cols, LANES)
        source = (self.io.w_beta, self.io.w_decay)[side]
        return pltpu.make_async_copy(
            source.at[:, pl.ds(start, self.block_cols)],
            self.refs.small_weights.at[side],
            self.refs.small_sem.at[side],
        )

    def start_fetches(self):
        self.fetch_small(0).start()
        self.fetch_small(1).start()

        def weights(j, carry):
            for side in range(4):
                self.fetch(j, side).start()
            self.fetch_mix(j).start()
            return carry

        def states(j, carry):
            self.fetch_state(j).start()
            return carry

        lax.fori_loop(0, self.heads, weights, 0)
        lax.fori_loop(0, self.slots, states, 0)

    def gates(self, totals, model_width):
        refs, io, heads = self.refs, self.io, self.heads
        all_heads = refs.small_weights.shape[1]
        block = totals.shape[0]
        row_scale = lax.rsqrt(
            totals[:, 2 * all_heads : 2 * all_heads + 1] / model_width + EPSILON
        )
        refs.row_scale[...] = jnp.broadcast_to(row_scale, (block, LANES))
        scaled_small = row_scale * totals
        lane = lax.broadcasted_iota(jnp.int32, (block, LANES), 1)
        own = lax.broadcasted_iota(jnp.int32, (block, block), 0) == lax.broadcasted_iota(
            jnp.int32, (block, block), 1
        )

        def stand(row):
            spread = jnp.broadcast_to(row, (block, block))
            return jnp.sum(jnp.where(own, spread, 0.0), axis=1, keepdims=True)

        span = jnp.floor(stand(io.lengths[...].astype(jnp.float32)) * (1.0 / SPAN))
        spans = io.span_bias.shape[1]
        matches = (
            lax.broadcasted_iota(jnp.int32, (block, spans), 1).astype(jnp.float32) == span
        )
        for h in range(heads):
            at = self.tp * heads + h
            beta_raw = jnp.sum(jnp.where(lane == at, scaled_small, 0.0), axis=1, keepdims=True)
            decay_raw = jnp.sum(
                jnp.where(lane == all_heads + at, scaled_small, 0.0), axis=1, keepdims=True
            )
            bias = jnp.sum(
                jnp.where(matches, io.span_bias[h : h + 1, :], 0.0), axis=1, keepdims=True
            )
            inner = decay_raw + io.decay_bias[:, h : h + 1] + bias
            soft = jnp.maximum(inner, 0.0) + jnp.log1p(jnp.exp(-jnp.abs(inner)))
            rate = jnp.exp(io.decay_rate[:, h : h + 1])
            decay = jnp.exp(-rate * soft + stand(io.extra[h : h + 1, :]))
            refs.decay[h] = jnp.broadcast_to(decay, (block, LANES))
            refs.beta[h] = jnp.broadcast_to(jax.nn.sigmoid(beta_raw), (block, LANES))

    def finish(self, j, sums):
        refs, io, size = self.refs, self.io, self.head_size
        block = sums.shape[0]

        def unit(raw):
            return raw * lax.rsqrt(jnp.sum(raw * raw, axis=1, keepdims=True) + EPSILON)

        sums = refs.row_scale[:, :1] * sums
        query = unit(jax.nn.silu(sums[:, :size])) * size ** (-0.5)
        key = unit(jax.nn.silu(sums[:, size : 2 * size]))
        value = jax.nn.silu(sums[:, 2 * size : 3 * size])
        gate = jax.nn.silu(sums[:, 3 * size :])
        refs.key[...] = key
        refs.value[...] = value
        refs.match[...] = jnp.broadcast_to(
            jnp.sum(key * query, axis=1, keepdims=True), (block, size)
        )
        refs.turned[...] = jnp.concatenate([key, query, value, gate], axis=0).T
        self.fetch_state(j).wait()
        slot = lax.rem(j, self.slots)
        for b in range(block):
            held = refs.state[slot, b]
            by_key = jnp.sum(held * refs.turned[:, b : b + 1], axis=0, keepdims=True)
            by_query = jnp.sum(
                held * refs.turned[:, block + b : block + b + 1], axis=0, keepdims=True
            )
            row = slice(b, b + 1)
            decay = refs.decay[j, row]
            write = refs.beta[j, row] * (refs.value[row] - decay * by_key)
            refs.readout[row] = decay * by_query + refs.match[row] * write
            io.decays[b, pl.ds(j, 1)] = decay
            io.keys[b, pl.ds(j, 1)] = refs.key[row]
            io.writes[b, pl.ds(j, 1)] = write

        @pl.when(j + self.slots < self.heads)
        def _():
            self.fetch_state(j + self.slots).start()

        readout = refs.readout[...]
        readout = (
            readout
            * lax.rsqrt(jnp.mean(readout * readout, axis=1, keepdims=True) + EPSILON)
            * io.head_gain[...]
            * gate
        )
        return readout.astype(jnp.bfloat16)

    def run(self, x, gain, model_width):
        refs, kv, n = self.refs, self.kv, self.n
        squares = scale_rows(x, gain, refs.scaled, kv)
        all_heads = refs.small_weights.shape[1]
        rows = squares.shape[0]
        small = refs.small
        small[...] = jnp.broadcast_to(squares, small.shape)
        for side in range(2):
            self.fetch_small(side).wait()
            small[:, side * all_heads : (side + 1) * all_heads] = lax.dot_general(
                refs.scaled[...],
                refs.small_weights[side],
                (((1,), (1,)), ((), ())),
                preferred_element_type=jnp.float32,
            )
        refs.row_part[...] = small[...].reshape(n, rows // n, LANES)
        row_copies = sum_rows_start(refs, kv, n)
        exchange = Exchange(refs, kv, n, self.heads, plain_share(n, self.heads))

        def product(j):
            for side in range(4):
                self.fetch(j, side).wait()
            return jnp.dot(
                refs.scaled[...], refs.weights[j], preferred_element_type=jnp.float32
            )

        exchange.produce(product)
        self.gates(sum_rows_finish(refs, row_copies, kv, n), model_width)
        exchange.run(self.finish)
        exchange.consume(refs.total, refs.mix_out, lambda j: self.fetch_mix(j).wait())

        def drain():
            exchange.drain()
            for copy in row_copies:
                copy.wait_send()

        return drain


def layer_kernel(model_width, aligned, io, refs):
    kv, tp = lax.axis_index(KV), lax.axis_index(TP)
    n, n_tp = lax.axis_size(KV), lax.axis_size(TP)
    feed, mix, blocks = refs.feed, refs.mix, refs.blocks
    half = blocks.shape[2]
    small_copies = []
    for item, (name, near) in enumerate(vars(refs.small).items()):
        copy = pltpu.make_async_copy(getattr(io, name), near, refs.small_sem.at[item])
        copy.start()
        small_copies.append(copy)
        setattr(io, name, near)
    if aligned:
        x_copies = [pltpu.make_async_copy(io.x, refs.pieces.at[tp], refs.x_sem.at[0])]
    else:
        x_copies = [
            pltpu.make_async_copy(
                io.x.at[pl.ds(side * half, half)], blocks.at[0, side], refs.x_sem.at[side]
            )
            for side in range(2)
        ]
    for copy in x_copies:
        copy.start()
    first = Feed(feed, (io.w_gate_one, io.w_up_one, io.w_down_one), kv, tp)
    second = Feed(feed, (io.w_gate_two, io.w_up_two, io.w_down_two), kv, tp)
    mixer = Mixer(mix, io, kv, tp)
    first.start_weights()
    meet(kv, tp, n, n_tp)
    for copy in x_copies:
        copy.wait()
    copies = []
    if aligned:
        own = io.x.shape[1]
        for away in range(1, n_tp):
            copy = to_tp(
                refs.pieces.at[tp],
                refs.pieces.at[tp],
                refs.piece_sem.at[0, away - 1],
                refs.piece_sem.at[1, away - 1],
                lax.rem(tp + away, n_tp),
            )
            copy.start()
            copies.append(copy)
    first.start_down()
    mixer.start_fetches()
    for copy in small_copies:
        copy.wait()
    for copy in copies:
        copy.wait_recv()
    if aligned:
        for piece in range(n_tp):
            columns = slice(piece * own, (piece + 1) * own)
            blocks[0, 0, :, columns] = refs.pieces[piece, :half]
            blocks[0, 1, :, columns] = refs.pieces[piece, half:]
    drain = first.run(blocks.at[0], io.gain_one, model_width)
    second.start_weights()
    second.start_down()
    copies += total_over_tp(
        refs.sums_one, feed.total, blocks.at[0], blocks.at[1], 0.5, tp, n_tp
    )
    drain_mixer = mixer.run(blocks.at[1], io.gain_mix, model_width)
    drain()
    copies += total_over_tp(refs.sums_mix, mix.total, blocks.at[1], blocks.at[2], 1.0, tp, n_tp)
    drain = second.run(blocks.at[2], io.gain_two, model_width)
    if aligned:
        copies += own_columns(refs, feed.total, blocks.at[2], io.out, tp, n_tp)
    else:
        copies += total_over_tp(refs.sums_two, feed.total, blocks.at[2], io.out, 0.5, tp, n_tp)
    drain()
    drain_mixer()
    for copy in copies:
        copy.wait_send()


def spaced(tree):
    if isinstance(tree, dict):
        return SimpleNamespace(**{name: spaced(leaf) for name, leaf in tree.items()})
    return tree


def call_kernel(kernel, inputs, outputs, scratch, name, call_id):
    arrays = [array for array, _ in inputs.values()]
    leaves, tree = jax.tree.flatten(scratch)

    def entry(*given):
        io = dict(zip([*inputs, *outputs], given))
        kernel(spaced(io), spaced(jax.tree.unflatten(tree, given[len(io) :])))

    return pl.pallas_call(
        entry,
        out_shape=[shape for shape, _ in outputs.values()],
        in_specs=[pl.BlockSpec(memory_space=space) for _, space in inputs.values()],
        out_specs=[pl.BlockSpec(memory_space=space) for _, space in outputs.values()],
        scratch_shapes=leaves,
        name=name,
        compiler_params=pltpu.CompilerParams(
            collective_id=call_id, has_side_effects=True, vmem_limit_bytes=LIMIT
        ),
    )(*arrays)


def row_scratch(scratch, rows, block_cols, n):
    scratch.scaled = pltpu.VMEM((rows, block_cols), jnp.bfloat16)
    scratch.row_scale = pltpu.VMEM((rows // n, LANES), jnp.float32)
    scratch.total = pltpu.VMEM((rows, block_cols), jnp.float32)
    return vars(scratch)


def layer(
    x,
    previous_state,
    lengths,
    gain_one,
    w_gate_one,
    w_up_one,
    w_down_one,
    gain_mix,
    w_query,
    w_key,
    w_value,
    w_gate,
    w_beta,
    w_decay,
    decay_rate,
    decay_bias,
    span_bias,
    extra,
    head_gain,
    w_mix,
    gain_two,
    w_gate_two,
    w_up_two,
    w_down_two,
    aligned,
):
    n, n_tp = lax.axis_size(KV), lax.axis_size(TP)
    rows = x.shape[0]
    block_cols, columns = w_gate_one.shape
    own = block_cols // n_tp
    block, heads, head_size = previous_state.shape[:3]
    all_heads = w_beta.shape[1]
    chunks = chunks_of(columns)
    width = columns // chunks
    vmem, hbm = pltpu.VMEM, pltpu.HBM

    def far(array):
        return (pltpu.with_memory_space_constraint(array, hbm), hbm)

    def row(array):
        return array.reshape(1, -1)

    small = dict(
        gain_one=row(gain_one),
        gain_mix=row(gain_mix),
        gain_two=row(gain_two),
        lengths=row(lengths),
        span_bias=span_bias,
        extra=extra.T,
        head_gain=row(head_gain),
        decay_rate=row(decay_rate),
        decay_bias=row(decay_bias),
    )
    inputs = dict(
        x=far(x),
        w_gate_one=far(w_gate_one),
        w_up_one=far(w_up_one),
        w_down_one=far(w_down_one),
        w_query=far(w_query),
        w_key=far(w_key),
        w_value=far(w_value),
        w_gate=far(w_gate),
        w_beta=far(w_beta.T),
        w_decay=far(w_decay.T),
        w_mix=far(w_mix),
        w_gate_two=far(w_gate_two),
        w_up_two=far(w_up_two),
        w_down_two=far(w_down_two),
        previous=far(previous_state),
        **{name: far(array) for name, array in small.items()},
    )
    shape = (rows, own) if aligned else (2, rows // 2, block_cols)
    rows_of_heads = jax.ShapeDtypeStruct((block, heads, head_size), jnp.float32)
    outputs = dict(
        out=(jax.ShapeDtypeStruct(shape, jnp.bfloat16), vmem),
        decays=(rows_of_heads, vmem),
        keys=(rows_of_heads, vmem),
        writes=(rows_of_heads, vmem),
    )
    feed = exchange_scratch(n, chunks, rows, 2 * width, width)
    feed.weights = vmem((chunks, block_cols, 2 * width), jnp.bfloat16)
    feed.down = vmem((chunks, width, block_cols), jnp.bfloat16)
    feed.weight_sem = pltpu.SemaphoreType.DMA((3, chunks))
    mix = exchange_scratch(n, heads, rows, 4 * head_size, head_size)
    mix.weights = vmem((heads, block_cols, 4 * head_size), jnp.bfloat16)
    mix.mix_out = vmem((heads, head_size, block_cols), jnp.bfloat16)
    mix.weight_sem = pltpu.SemaphoreType.DMA((5, heads))
    mix.state = vmem((min(heads, 4), block, head_size, head_size), jnp.float32)
    mix.state_sem = pltpu.SemaphoreType.DMA((heads,))
    mix.small_weights = vmem((2, all_heads, block_cols), jnp.bfloat16)
    mix.small_sem = pltpu.SemaphoreType.DMA((2,))
    mix.small = vmem((rows, LANES), jnp.float32)
    mix.decay = vmem((heads, block, LANES), jnp.float32)
    mix.beta = vmem((heads, block, LANES), jnp.float32)
    mix.key = vmem((block, head_size), jnp.float32)
    mix.value = vmem((block, head_size), jnp.float32)
    mix.match = vmem((block, head_size), jnp.float32)
    mix.readout = vmem((block, head_size), jnp.float32)
    mix.turned = vmem((head_size, 4 * block), jnp.float32)
    scratch = dict(
        feed=row_scratch(feed, rows, block_cols, n),
        mix=row_scratch(mix, rows, block_cols, n),
        blocks=vmem((3, 2, rows // 2, block_cols), jnp.bfloat16),
        sums_one=tp_scratch(n_tp, rows, block_cols),
        sums_mix=tp_scratch(n_tp, rows, block_cols),
        small={name: vmem(array.shape, array.dtype) for name, array in small.items()},
        small_sem=pltpu.SemaphoreType.DMA((len(small),)),
        x_sem=pltpu.SemaphoreType.DMA((2,)),
    )
    if aligned:
        scratch.update(
            pieces=vmem((n_tp, rows, own), jnp.bfloat16),
            piece_sem=pltpu.SemaphoreType.DMA((2, n_tp - 1)),
            out_part=vmem((n_tp, rows, own), jnp.bfloat16),
            out_slot=vmem((n_tp - 1, rows, own), jnp.bfloat16),
            out_sem=pltpu.SemaphoreType.DMA((2, n_tp - 1)),
        )
    else:
        scratch.update(sums_two=tp_scratch(n_tp, rows, block_cols))
    out, decays, keys, writes = call_kernel(
        functools.partial(layer_kernel, gain_one.shape[0], aligned),
        inputs,
        outputs,
        scratch,
        "layer",
        0,
    )
    return out if aligned else out.reshape(rows, block_cols), decays, keys, writes


def body(
    tokens,
    previous_state,
    lengths,
    first_feed_norm_gain,
    first_gate_projection,
    first_up_projection,
    first_down_projection,
    mixer_norm_gain,
    query_weight,
    key_weight,
    value_weight,
    output_gate_weight,
    write_strength_weight,
    decay_input_weight,
    head_log_decay_rate,
    decay_input_bias,
    length_span_bias,
    extra_log_decay,
    readout_head_norm_gain,
    mixer_output_weight,
    second_feed_norm_gain,
    second_gate_projection,
    second_up_projection,
    second_down_projection,
):
    own_cols = tokens.shape[1]
    aligned = own_cols % LANES == 0
    if not aligned:
        tokens = lax.all_gather(tokens, TP, axis=1, tiled=True)
    result, decays, keys, writes = layer(
        tokens,
        previous_state,
        lengths,
        first_feed_norm_gain,
        first_gate_projection,
        first_up_projection,
        first_down_projection,
        mixer_norm_gain,
        query_weight,
        key_weight,
        value_weight,
        output_gate_weight,
        write_strength_weight,
        decay_input_weight,
        head_log_decay_rate,
        decay_input_bias,
        length_span_bias,
        extra_log_decay,
        readout_head_norm_gain,
        mixer_output_weight,
        second_feed_norm_gain,
        second_gate_projection,
        second_up_projection,
        second_down_projection,
        aligned,
    )
    new_state = (
        decays[:, :, None, :] * previous_state + keys[:, :, :, None] * writes[:, :, None, :]
    )
    if not aligned:
        start = lax.axis_index(TP) * own_cols
        result = lax.dynamic_slice_in_dim(result, start, own_cols, 1)
    return (result, new_state)


def solution(mesh):
    return jax.shard_map(
        body,
        mesh=mesh,
        in_specs=(
            P(None, (KV, TP)),
            P(KV, TP, None, None),
            P(KV),
            P(),
            P(KV, TP),
            P(KV, TP),
            P(TP, KV),
            P(),
            P(KV, TP),
            P(KV, TP),
            P(KV, TP),
            P(KV, TP),
            P(),
            P(),
            P(TP),
            P(TP),
            P(TP, None),
            P(KV, TP),
            P(),
            P(TP, KV),
            P(),
            P(KV, TP),
            P(KV, TP),
            P(TP, KV),
        ),
        out_specs=(P(None, (KV, TP)), P(KV, TP, None, None)),
        check_vma=False,
    )
```

time: 429 us -> 194 us (0.45); the launches traced: 421 us -> 193 us
  Pallas kernels: 322 us -> 185 us
  matrix products: 61 us -> 0 us
  other arithmetic: 21.9 us -> 6.67 us
  blocking collectives: 7.45 us -> 0 us
  local copies, waits for them, and re-layouts: 7 us -> 0.63 us
    pallas_call x9 -> x1, Pallas kernels: 322 us -> 185 us  [call_kernel(): pl.pallas_call(entry, out_shape=[shape for shape, _ in outputs.values()],...]
    dot_general x15 -> x0, matrix products: 61 us -> none  [the longest x1 18.4 us: body(): jnp.einsum('bhkv,bhk->bhv', held_state, key_heads, precision=lax.Precisio...]
    all_gather x1 -> x0, blocking collectives: 7.45 us -> none  [body(): token_block = lax.all_gather(tokens, 'tp', axis=1, tiled=True)]
    convert_element_type x4 -> x0, other arithmetic: 5.57 us -> none  [the longest x2 3.9 us: ffn_block(): (jax.nn.silu(row_scale * gate_share) * (row_scale * up_share)).astype(jnp...]
where the time goes in v1:
time: 194 us; the launch traced here: 193 us
  Pallas kernels  185 us (95%)
  other arithmetic  6.67 us (3%)
    pallas_call x1, Pallas kernels, call_kernel(): pl.pallas_call(entry, out_shape=[shape for shape, _ in outputs.values()],...  185 us
    add x1, other arithmetic, body(): decays[:, :, None, :] * previous_state  6.67 us

profile of v1, /device:TPU:1, one launch (start us, length us, event | category | flops | bytes accessed | tf_op | source)
XLA Modules:
  0.0 193.4 jit_solution(12755798641903432887)
XLA Ops:
  0.6 0.0 copy-start
  0.7 185.4 %layer.1 = (bf16[256,128]{1,0:T(8,128)(2,1)S(1)}, f32[32,8,128]{2,1,0:T(8,128)S(1)}, f32[32,8,128]{2,1,0:T(8,128)S(1)}, f32[32,8,128]{2,1,0:T(8,128)S(1)}) custom-call(bf16[256,128]{1,0:T(8,128)(2,1)} %given_0_.1, bf16[512,2816]{1,0:T(8,128)(2,1)} %given_1_.1, bf16[512,2816]{1,0:T(8,128)(2,1)} %given_2_.1, bf16[2816,512]{1,0:T(8,128)(2,1)} %given_3_.1, ...), custom_call_target="tpu_custom_call" | custom-call | tf_op jit(solution)/shard_map/layer/pallas_call | solution.py:705
  186.1 0.0 copy-done
  186.1 6.7 %multiply_add_fusion = f32[32,8,128,128]{3,2,1,0:T(8,128)} fusion(f32[32,8,128,128]{3,2,1,0:T(8,128)S(1)} %copy-done, f32[32,8,128]{2,1,0:T(8,128)S(1)} %get-tuple-element.9, f32[32,8,128]{2,1,0:T(8,128)S(1)} %get-tuple-element.8, f32[32,8,128]{2,1,0:T(8,128)S(1)} %get-tuple-element.7), kind=kLoop, calls=%fused_computation | loop fusion | flops 12582912 | bytes 33947648 | tf_op jit(solution)/shard_map/add | solution.py:914
  192.7 0.6 copy.27
Async XLA Ops:
  0.6 185.4 %copy-start = (f32[32,8,128,128]{3,2,1,0:T(8,128)S(1)}, f32[32,8,128,128]{3,2,1,0:T(8,128)}, u32[]{:S(2)}) copy-start(f32[32,8,128,128]{3,2,1,0:T(8,128)} %given_14_.1) | copy-start | bytes 50331652

commit v2 on v1

--- a/solution.py
+++ b/solution.py
@@ -20,6 +20,9 @@
 LIMIT = 46 << 20
 
 
+PIECES = 2
+
+
 KV = "kv"
 
 
@@ -37,16 +40,13 @@
     return lax.rem(value // (1 << place), 2)
 
 
-def orders(n):
-    bits = log2(n)
-    plain = tuple(range(bits))
-    swapped = (1, 0) + tuple(range(2, bits)) if bits > 1 else plain
-    return plain, swapped
-
-
-def place_of(block, order):
-    bits = len(order)
-    return sum(((block >> b) & 1) << (bits - 1 - k) for k, b in enumerate(order))
+def place_of(block, bits):
+    return sum(((block >> k) & 1) << (bits - 1 - k) for k in range(bits))
+
+
+def groups(n):
+    near = max(n // 4, 2)
+    return near, n // near
 
 
 def meet(kv, tp, n_kv, n_tp):
@@ -110,79 +110,72 @@
 
 
 class Exchange:
-    def __init__(self, refs, kv, n, chunks, plain_chunks):
-        self.refs, self.kv, self.n = refs, kv, n
-        self.chunks, self.plain_chunks = chunks, plain_chunks
+    def __init__(self, refs, kv, n, chunks):
+        self.refs, self.chunks, self.kv, self.n = refs, chunks, kv, n
         self.bits = log2(n)
-        self.orders = orders(n)
-
-    def mine(self, j, k):
-        first, second = self.orders[0][k], self.orders[1][k]
-        if first == second:
-            return bit(self.kv, first)
-        return jnp.where(j < self.plain_chunks, bit(self.kv, first), bit(self.kv, second))
-
-    def peer(self, j, k):
-        first, second = self.orders[0][k], self.orders[1][k]
-        up = self.kv + (1 - 2 * bit(self.kv, first)) * (1 << first)
-        if first == second:
-            return up
-        other = self.kv + (1 - 2 * bit(self.kv, second)) * (1 << second)
-        return jnp.where(j < self.plain_chunks, up, other)
-
-    def place(self, depth):
-        total = 0
-        for k in range(depth):
-            total = total + bit(self.kv, k) * (self.n >> (k + 1))
-        return total
+        self.near, self.far = groups(n)
+        self.outer, self.inner = kv // self.near, lax.rem(kv, self.near)
+
+    def inner_peer(self, away):
+        return lax.rem(self.inner + away, self.near)
+
+    def outer_peer(self, away):
+        return sum(
+            lax.rem(bit(self.outer, k) + (away >> k), 2) * (1 << k)
+            for k in range(log2(self.far))
+        )
 
     def scatter(self, j, k):
+        side = bit(self.kv, k)
         return to_kv(
-            self.refs.part[k].at[j, 1 - self.mine(j, k)],
+            self.refs.part[k].at[j, 1 - side],
             self.refs.slot[k].at[j],
             self.refs.scatter_sem.at[0, k, j],
             self.refs.scatter_sem.at[1, k, j],
-            self.peer(j, k),
-        )
-
-    def gather(self, j, a):
-        last = self.bits - 1 - a
-        window = self.refs.full.at[j, pl.ds(self.place(self.bits - a), 1 << a)]
+            self.kv + (1 - 2 * side) * (1 << k),
+        )
+
+    def gather_far(self, j, away):
+        own = self.refs.full.at[j, self.inner, self.outer]
+        return to_kv(
+            own,
+            own,
+            self.refs.back_sem.at[0, away - 1, j],
+            self.refs.back_sem.at[1, away - 1, j],
+            self.outer_peer(away) * self.near + self.inner,
+        )
+
+    def gather_near(self, j, away):
+        window = self.refs.full.at[j, self.inner]
         return to_kv(
             window,
             window,
-            self.refs.gather_sem.at[0, a, j],
-            self.refs.gather_sem.at[1, a, j],
-            self.kv + (1 - 2 * bit(self.kv, last)) * (1 << last),
+            self.refs.relay_sem.at[0, away - 1, j],
+            self.refs.relay_sem.at[1, away - 1, j],
+            self.outer * self.near + self.inner_peer(away),
         )
 
     def produce(self, product):
+        part = self.refs.part[0]
         rows = self.refs.slot[-1].shape[1]
-        part = self.refs.part[0]
         half = self.n // 2
-        for order, low, high in (
-            (self.orders[0], 0, 1),
-            (self.orders[1], self.plain_chunks, self.chunks),
-            (self.orders[0], 1, self.plain_chunks),
-        ):
-
-            def step(j, carry, order=order):
-                value = product(j)
-                for block in range(self.n):
-                    place = place_of(block, order)
-                    start = (place % half) * rows
-                    part[j, place // half, start : start + rows] = value[
-                        block * rows : (block + 1) * rows
-                    ].astype(part.dtype)
-                self.scatter(j, 0).start()
-                return carry
-
-            if high > low:
-                lax.fori_loop(low, high, step, 0)
+
+        def step(j, carry):
+            value = product(j)
+            for block in range(self.n):
+                place = place_of(block, self.bits)
+                start = place % half * rows
+                part[j, place // half, start : start + rows] = value[
+                    block * rows : (block + 1) * rows
+                ].astype(part.dtype)
+            self.scatter(j, 0).start()
+            return carry
+
+        lax.fori_loop(0, self.chunks, step, 0)
 
     def reduce(self, j, k, finish):
         self.scatter(j, k - 1).wait_recv()
-        total = self.refs.part[k - 1][j, self.mine(j, k - 1)].astype(jnp.float32)
+        total = self.refs.part[k - 1][j, bit(self.kv, k - 1)].astype(jnp.float32)
         total = total + self.refs.slot[k - 1][j].astype(jnp.float32)
         if k < self.bits:
             part = self.refs.part[k]
@@ -190,57 +183,49 @@
             part[j, 0] = total[:rows].astype(part.dtype)
             part[j, 1] = total[rows:].astype(part.dtype)
             self.scatter(j, k).start()
-        else:
-            full = self.refs.full
-            full[j, self.place(self.bits)] = finish(j, total)
-            self.gather(j, 0).start()
-
-    def relay(self, j, a):
-        self.gather(j, a - 1).wait_recv()
-        self.gather(j, a).start()
+            return
+        self.refs.full[j, self.inner, self.outer] = finish(j, total)
+        for away in range(1, self.far):
+            self.gather_far(j, away).start()
+
+    def relay(self, j):
+        for back in range(1, self.far):
+            self.gather_far(j, back).wait_recv()
+        for away in range(1, self.near):
+            self.gather_near(j, away).start()
 
     def run(self, finish):
-        bits = self.bits
-
         def step(t, carry):
-            @pl.when(t < self.plain_chunks)
-            def _():
-                self.reduce(t, 1, finish)
-
-            @pl.when(t < self.chunks - self.plain_chunks)
-            def _():
-                self.reduce(self.plain_chunks + t, 1, finish)
-
-            for lag in range(1, 2 * bits - 1):
+            for lag in range(self.bits + 1):
                 j = t - lag
 
                 @pl.when(jnp.logical_and(j >= 0, j < self.chunks))
                 def _(lag=lag, j=j):
-                    if lag < bits:
+                    if lag < self.bits:
                         self.reduce(j, lag + 1, finish)
                     else:
-                        self.relay(j, lag - bits + 1)
+                        self.relay(j)
 
             return carry
 
-        lax.fori_loop(0, self.chunks + 2 * bits - 2, step, 0)
+        lax.fori_loop(0, self.chunks + self.bits, step, 0)
 
     def consume(self, total, weight, weight_wait):
         full = self.refs.full
-        rows, width = full.shape[2], full.shape[3]
+        rows, width = full.shape[3:]
         total[...] = jnp.zeros_like(total)
-        order = self.orders[0]
 
         def step(j, carry):
             weight_wait(j)
-            self.gather(j, self.bits - 1).wait_recv()
+            for away in range(1, self.near):
+                self.gather_near(j, away).wait_recv()
             product = jnp.dot(
-                full[j].reshape(self.n * rows, width),
+                full[j].reshape(self.near * self.far * rows, width),
                 weight[j],
                 preferred_element_type=jnp.float32,
             )
-            for block in range(self.n):
-                place = place_of(block, order)
+            for block in range(self.near * self.far):
+                place = block % self.near * self.far + block // self.near
                 total[block * rows : (block + 1) * rows] += product[
                     place * rows : (place + 1) * rows
                 ]
@@ -250,56 +235,79 @@
 
     def drain(self):
         def step(j, carry):
+            for away in range(1, self.near):
+                self.gather_near(j, away).wait_send()
+            for away in range(1, self.far):
+                self.gather_far(j, away).wait_send()
             for k in range(self.bits):
                 self.scatter(j, k).wait_send()
-                self.gather(j, k).wait_send()
             return carry
 
         lax.fori_loop(0, self.chunks, step, 0)
 
 
 def total_over_tp(refs, total, base, out, scale, tp, n_tp):
+    part, slot, sems = refs.tp_part, refs.tp_slot, refs.tp_sem
+    pieces, rows = part.shape[1], part.shape[3]
     half = total.shape[0] // 2
     core = bit(tp, 0)
     other = tp + 1 - 2 * core
-    part, slot, sems = refs.tp_part, refs.tp_slot, refs.tp_sem
-    part[0, 0] = total[:half].astype(part.dtype)
-    part[0, 1] = total[half:].astype(part.dtype)
-    copies = [to_tp(part.at[0, 1 - core], slot.at[0], sems.at[0, 0], sems.at[1, 0], other)]
-    copies[-1].start()
-    copies[-1].wait_recv()
-    value = part[0, core].astype(jnp.float32) + slot[0].astype(jnp.float32)
-    for place in range(1, log2(n_tp)):
-        part[place, 0] = value.astype(part.dtype)
-        peer = tp + (1 - 2 * bit(tp, place)) * (1 << place)
-        copies.append(
-            to_tp(part.at[place, 0], slot.at[place], sems.at[0, place], sems.at[1, place], peer)
-        )
-        copies[-1].start()
-        copies[-1].wait_recv()
-        value = part[place, 0].astype(jnp.float32) + slot[place].astype(jnp.float32)
-    out[core] = (base[core].astype(jnp.float32) + scale * value).astype(out.dtype)
     last = log2(n_tp)
-    copies.append(to_tp(out.at[core], out.at[core], sems.at[0, last], sems.at[1, last], other))
-    copies[-1].start()
-    copies[-1].wait_recv()
+    copies = []
+
+    def send(src, dst, place, piece, peer):
+        copy = to_tp(src, dst, sems.at[0, place, piece], sems.at[1, place, piece], peer)
+        copy.start()
+        copies.append(copy)
+        return copy
+
+    def window(piece):
+        return pl.ds(piece * rows, rows)
+
+    flying = []
+    for piece in range(pieces):
+        for side in range(2):
+            start = side * half + piece * rows
+            part[0, piece, side] = total[start : start + rows].astype(part.dtype)
+        flying.append(
+            send(part.at[0, piece, 1 - core], slot.at[0, piece], 0, piece, other)
+        )
+    for place in range(1, last + 1):
+        for piece in range(pieces):
+            flying[piece].wait_recv()
+            own = part[0, piece, core] if place == 1 else part[place - 1, piece, 0]
+            value = own.astype(jnp.float32) + slot[place - 1, piece].astype(jnp.float32)
+            if place < last:
+                part[place, piece, 0] = value.astype(part.dtype)
+                peer = tp + (1 - 2 * bit(tp, place)) * (1 << place)
+                flying[piece] = send(
+                    part.at[place, piece, 0], slot.at[place, piece], place, piece, peer
+                )
+            else:
+                kept = base[core, window(piece)].astype(jnp.float32)
+                out[core, window(piece)] = (kept + scale * value).astype(out.dtype)
+                rows_out = out.at[core, window(piece)]
+                flying[piece] = send(rows_out, rows_out, last, piece, other)
+    for copy in flying:
+        copy.wait_recv()
     return copies
 
 
-def exchange_scratch(n, chunks, rows, cols, width):
-    bits = log2(n)
+def exchange_scratch(n, chunks, rows, cols, width, row_shape):
+    near, far = groups(n)
     shapes = SimpleNamespace()
     shapes.part = [
-        pltpu.VMEM((chunks, 2, rows >> (k + 1), cols), jnp.bfloat16) for k in range(bits)
+        pltpu.VMEM((chunks, 2, rows >> (k + 1), cols), jnp.bfloat16) for k in range(log2(n))
     ]
     shapes.slot = [
-        pltpu.VMEM((chunks, rows >> (k + 1), cols), jnp.bfloat16) for k in range(bits)
+        pltpu.VMEM((chunks, rows >> (k + 1), cols), jnp.bfloat16) for k in range(log2(n))
     ]
-    shapes.full = pltpu.VMEM((chunks, n, rows // n, width), jnp.bfloat16)
-    shapes.scatter_sem = pltpu.SemaphoreType.DMA((2, bits, chunks))
-    shapes.gather_sem = pltpu.SemaphoreType.DMA((2, bits, chunks))
-    shapes.row_part = pltpu.VMEM((n, rows // n, LANES), jnp.float32)
-    shapes.row_slot = pltpu.VMEM((n - 1, rows // n, LANES), jnp.float32)
+    shapes.full = pltpu.VMEM((chunks, near, far, rows // n, width), jnp.bfloat16)
+    shapes.scatter_sem = pltpu.SemaphoreType.DMA((2, log2(n), chunks))
+    shapes.back_sem = pltpu.SemaphoreType.DMA((2, far - 1, chunks))
+    shapes.relay_sem = pltpu.SemaphoreType.DMA((2, near - 1, chunks))
+    shapes.row_part = pltpu.VMEM((n,) + row_shape, jnp.float32)
+    shapes.row_slot = pltpu.VMEM((n - 1,) + row_shape, jnp.float32)
     shapes.row_sem = pltpu.SemaphoreType.DMA((2, n - 1))
     return shapes
 
@@ -307,9 +315,9 @@
 def tp_scratch(n_tp, rows, cols):
     bits = log2(n_tp)
     return dict(
-        tp_part=pltpu.VMEM((bits, 2, rows // 2, cols), jnp.bfloat16),
-        tp_slot=pltpu.VMEM((bits, rows // 2, cols), jnp.bfloat16),
-        tp_sem=pltpu.SemaphoreType.DMA((2, bits + 1)),
+        tp_part=pltpu.VMEM((bits, PIECES, 2, rows // 2 // PIECES, cols), jnp.bfloat16),
+        tp_slot=pltpu.VMEM((bits, PIECES, rows // 2 // PIECES, cols), jnp.bfloat16),
+        tp_sem=pltpu.SemaphoreType.DMA((2, bits + 1, PIECES)),
     )
 
 
@@ -318,8 +326,15 @@
     return max(d for d in range(1, 13) if tiles % d == 0)
 
 
-def plain_share(n, chunks):
-    return chunks if log2(n) < 2 else chunks - (chunks + 2) // 6
+def diagonal(size):
+    rows = lax.broadcasted_iota(jnp.int32, (size, size), 0)
+    return rows == lax.broadcasted_iota(jnp.int32, (size, size), 1)
+
+
+def turn(values, axis):
+    size = max(values.shape)
+    spread = jnp.broadcast_to(values, (size, size))
+    return jnp.sum(jnp.where(diagonal(size), spread, 0.0), axis=axis, keepdims=True)
 
 
 def scale_rows(x, gain, scaled, kv):
@@ -373,11 +388,12 @@
         refs, kv, n, width = self.refs, self.kv, self.n, self.width
         squares = scale_rows(x, gain, refs.scaled, kv)
         rows = squares.shape[0]
-        refs.row_part[...] = jnp.broadcast_to(squares, (rows, LANES)).reshape(
-            n, rows // n, LANES
-        )
+        block = rows // n
+        for peer in range(n):
+            row = turn(squares[peer * block : (peer + 1) * block], 0)
+            refs.row_part[peer, :, :block] = jnp.broadcast_to(row, (8, block))
         row_copies = sum_rows_start(refs, kv, n)
-        exchange = Exchange(refs, kv, n, self.chunks, plain_share(n, self.chunks))
+        exchange = Exchange(refs, kv, n, self.chunks)
 
         def product(j):
             self.fetch(j, 0).wait()
@@ -388,7 +404,8 @@
 
         exchange.produce(product)
         totals = sum_rows_finish(refs, row_copies, kv, n)
-        refs.row_scale[...] = lax.rsqrt(totals / model_width + EPSILON)
+        row_scale = lax.rsqrt(turn(totals[:1, :block], 1) / model_width + EPSILON)
+        refs.row_scale[...] = jnp.broadcast_to(row_scale, (block, LANES))
 
         def finish(j, sums):
             row_scale = refs.row_scale[:, :1]
@@ -500,15 +517,7 @@
         refs.row_scale[...] = jnp.broadcast_to(row_scale, (block, LANES))
         scaled_small = row_scale * totals
         lane = lax.broadcasted_iota(jnp.int32, (block, LANES), 1)
-        own = lax.broadcasted_iota(jnp.int32, (block, block), 0) == lax.broadcasted_iota(
-            jnp.int32, (block, block), 1
-        )
-
-        def stand(row):
-            spread = jnp.broadcast_to(row, (block, block))
-            return jnp.sum(jnp.where(own, spread, 0.0), axis=1, keepdims=True)
-
-        span = jnp.floor(stand(io.lengths[...].astype(jnp.float32)) * (1.0 / SPAN))
+        span = jnp.floor(turn(io.lengths[...].astype(jnp.float32), 1) * (1.0 / SPAN))
         spans = io.span_bias.shape[1]
         matches = (
             lax.broadcasted_iota(jnp.int32, (block, spans), 1).astype(jnp.float32) == span
@@ -525,7 +534,7 @@
             inner = decay_raw + io.decay_bias[:, h : h + 1] + bias
             soft = jnp.maximum(inner, 0.0) + jnp.log1p(jnp.exp(-jnp.abs(inner)))
             rate = jnp.exp(io.decay_rate[:, h : h + 1])
-            decay = jnp.exp(-rate * soft + stand(io.extra[h : h + 1, :]))
+            decay = jnp.exp(-rate * soft + turn(io.extra[h : h + 1, :], 1))
             refs.decay[h] = jnp.broadcast_to(decay, (block, LANES))
             refs.beta[h] = jnp.broadcast_to(jax.nn.sigmoid(beta_raw), (block, LANES))
 
@@ -593,7 +602,7 @@
             )
         refs.row_part[...] = small[...].reshape(n, rows // n, LANES)
         row_copies = sum_rows_start(refs, kv, n)
-        exchange = Exchange(refs, kv, n, self.heads, plain_share(n, self.heads))
+        exchange = Exchange(refs, kv, n, self.heads)
 
         def product(j):
             for side in range(4):
@@ -802,11 +811,11 @@
         keys=(rows_of_heads, vmem),
         writes=(rows_of_heads, vmem),
     )
-    feed = exchange_scratch(n, chunks, rows, 2 * width, width)
+    feed = exchange_scratch(n, chunks, rows, 2 * width, width, (8, LANES))
     feed.weights = vmem((chunks, block_cols, 2 * width), jnp.bfloat16)
     feed.down = vmem((chunks, width, block_cols), jnp.bfloat16)
     feed.weight_sem = pltpu.SemaphoreType.DMA((3, chunks))
-    mix = exchange_scratch(n, heads, rows, 4 * head_size, head_size)
+    mix = exchange_scratch(n, heads, rows, 4 * head_size, head_size, (block, LANES))
     mix.weights = vmem((heads, block_cols, 4 * head_size), jnp.bfloat16)
     mix.mix_out = vmem((heads, head_size, block_cols), jnp.bfloat16)
     mix.weight_sem = pltpu.SemaphoreType.DMA((5, heads))

time: 194 us -> 187 us (0.964)
  Pallas kernels: 185 us -> 179 us
    pallas_call x1, Pallas kernels: 185 us -> 179 us  [call_kernel(): pl.pallas_call(entry, out_shape=[shape for shape, _ in outputs.values()],...]
where the time goes in v2:
time: 187 us
  Pallas kernels  179 us (96%)
  other arithmetic  6.67 us (4%)
    pallas_call x1, Pallas kernels, call_kernel(): pl.pallas_call(entry, out_shape=[shape for shape, _ in outputs.values()],...  179 us
    add x1, other arithmetic, body(): decays[:, :, None, :] * previous_state  6.67 us

profile of v2, /device:TPU:1, one launch (start us, length us, event | category | flops | bytes accessed | tf_op | source)
XLA Modules:
  0.0 187.3 jit_solution(15644273252386406419)
XLA Ops:
  0.6 0.0 copy-start
  0.7 179.3 %layer.1 = (bf16[256,128]{1,0:T(8,128)(2,1)S(1)}, f32[32,8,128]{2,1,0:T(8,128)S(1)}, f32[32,8,128]{2,1,0:T(8,128)S(1)}, f32[32,8,128]{2,1,0:T(8,128)S(1)}) custom-call(bf16[256,128]{1,0:T(8,128)(2,1)} %given_0_.1, bf16[512,2816]{1,0:T(8,128)(2,1)} %given_1_.1, bf16[512,2816]{1,0:T(8,128)(2,1)} %given_2_.1, bf16[2816,512]{1,0:T(8,128)(2,1)} %given_3_.1, ...), custom_call_target="tpu_custom_call" | custom-call | tf_op jit(solution)/shard_map/layer/pallas_call | solution.py:714
  180.0 0.0 copy-done
  180.0 6.7 %multiply_add_fusion = f32[32,8,128,128]{3,2,1,0:T(8,128)} fusion(f32[32,8,128,128]{3,2,1,0:T(8,128)S(1)} %copy-done, f32[32,8,128]{2,1,0:T(8,128)S(1)} %get-tuple-element.9, f32[32,8,128]{2,1,0:T(8,128)S(1)} %get-tuple-element.8, f32[32,8,128]{2,1,0:T(8,128)S(1)} %get-tuple-element.7), kind=kLoop, calls=%fused_computation | loop fusion | flops 12582912 | bytes 33947648 | tf_op jit(solution)/shard_map/add | solution.py:923
  186.7 0.6 copy.27
Async XLA Ops:
  0.6 179.4 %copy-start = (f32[32,8,128,128]{3,2,1,0:T(8,128)S(1)}, f32[32,8,128,128]{3,2,1,0:T(8,128)}, u32[]{:S(2)}) copy-start(f32[32,8,128,128]{3,2,1,0:T(8,128)} %given_14_.1) | copy-start | bytes 50331652

commit v3 on v2

--- a/solution.py
+++ b/solution.py
@@ -21,6 +21,9 @@
 
 
 PIECES = 2
+
+
+SKEW = 2
 
 
 KV = "kv"
@@ -197,7 +200,7 @@
     def run(self, finish):
         def step(t, carry):
             for lag in range(self.bits + 1):
-                j = t - lag
+                j = t - SKEW * lag
 
                 @pl.when(jnp.logical_and(j >= 0, j < self.chunks))
                 def _(lag=lag, j=j):
@@ -208,7 +211,7 @@
 
             return carry
 
-        lax.fori_loop(0, self.chunks + self.bits, step, 0)
+        lax.fori_loop(0, self.chunks + SKEW * self.bits, step, 0)
 
     def consume(self, total, weight, weight_wait):
         full = self.refs.full

time: 187 us -> 188 us (level)
  no operation moved by 1% of the time
where the time goes in v3:
time: 188 us
  Pallas kernels  180 us (96%)
  other arithmetic  6.67 us (4%)
    pallas_call x1, Pallas kernels, call_kernel(): pl.pallas_call(entry, out_shape=[shape for shape, _ in outputs.values()],...  180 us
    add x1, other arithmetic, body(): decays[:, :, None, :] * previous_state  6.67 us

profile of v3, /device:TPU:1, one launch (start us, length us, event | category | flops | bytes accessed | tf_op | source)
XLA Modules:
  0.0 188.1 jit_solution(13223436945614664295)
XLA Ops:
  0.6 0.0 copy-start
  0.7 180.1 %layer.1 = (bf16[256,128]{1,0:T(8,128)(2,1)S(1)}, f32[32,8,128]{2,1,0:T(8,128)S(1)}, f32[32,8,128]{2,1,0:T(8,128)S(1)}, f32[32,8,128]{2,1,0:T(8,128)S(1)}) custom-call(bf16[256,128]{1,0:T(8,128)(2,1)} %given_0_.1, bf16[512,2816]{1,0:T(8,128)(2,1)} %given_1_.1, bf16[512,2816]{1,0:T(8,128)(2,1)} %given_2_.1, bf16[2816,512]{1,0:T(8,128)(2,1)} %given_3_.1, ...), custom_call_target="tpu_custom_call" | custom-call | tf_op jit(solution)/shard_map/layer/pallas_call | solution.py:717
  180.8 0.0 copy-done
  180.8 6.7 %multiply_add_fusion = f32[32,8,128,128]{3,2,1,0:T(8,128)} fusion(f32[32,8,128,128]{3,2,1,0:T(8,128)S(1)} %copy-done, f32[32,8,128]{2,1,0:T(8,128)S(1)} %get-tuple-element.9, f32[32,8,128]{2,1,0:T(8,128)S(1)} %get-tuple-element.8, f32[32,8,128]{2,1,0:T(8,128)S(1)} %get-tuple-element.7), kind=kLoop, calls=%fused_computation | loop fusion | flops 12582912 | bytes 33947648 | tf_op jit(solution)/shard_map/add | solution.py:926
  187.5 0.6 copy.27
Async XLA Ops:
  0.6 180.2 %copy-start = (f32[32,8,128,128]{3,2,1,0:T(8,128)S(1)}, f32[32,8,128,128]{3,2,1,0:T(8,128)}, u32[]{:S(2)}) copy-start(f32[32,8,128,128]{3,2,1,0:T(8,128)} %given_14_.1) | copy-start | bytes 50331652
